TPU v7x, 512 devices: a whole 4x8x8 slice. The times are simulated.
512 devices in a mesh: fs: 64 (over z, y), tp: 8 (over x, core).
Axes of the slice: x: 4, y: 8, z: 8, core: 2. Of those that a mesh axis runs over, the one named last changes fastest.
Arguments:
- saved_input: bfloat16 [65536, 2048], P('fs'), may hold values from -60 to 60
- out_cotangent: bfloat16 [65536, 4096], P('fs', 'tp'), may hold values from -6 to 6
- old_weight: float32 [2048, 4096], P('fs', 'tp'), may hold values from -0.125 to 0.125
- factor: bfloat16 [4096, 256], P('tp'), may hold values from -0.09375 to 0.09375
- moment_first: float32 [2048, 256], P('fs'), may hold values from -3 to 3
- moment_second: float32 [2048, 256], P('fs'), may hold values from 0.05 to 1
Outputs:
- new_weight: float32 [2048, 4096], P('fs', 'tp')
- update: float32 [2048, 4096], P('fs', 'tp')
- new_first: float32 [2048, 256], P('fs')
- new_second: float32 [2048, 256], P('fs')
- weight_copy: bfloat16 [2048, 4096], P(None, 'tp')
All inputs are finite; a program needn't handle non-finite values.
Results may differ from a plain program's by a relative error of at most 0.0028.
Values may be sent and summed in bfloat16 or wider, within the bound.
No kernel may reach another device: no remote copies, remote signals or barrier semaphores. Data moves between devices by JAX's collectives and lax.ppermute only.
A program may use at most 64 MiB of HBM per device.

v0:
```python
import math

import jax
import jax.numpy as jnp
from jax import lax
from jax.experimental import pallas as pl
from jax.sharding import Mesh
from jax.sharding import PartitionSpec as P

HV = 2048
RANK = 256
FS = ("fs_0", "fs_1")
LIMIT = math.sqrt(HV * RANK)


def exchanged(blocks, axis):
    return lax.all_to_all(blocks, axis, 0, 0, tiled=True)


def copy_for_each(shard, axis):
    devices = lax.axis_size(axis)
    return exchanged(jnp.broadcast_to(shard[None], (devices, *shard.shape)), axis)


def in_two(values):
    high = lax.reduce_precision(values, 8, 7)
    return high.astype(jnp.bfloat16), (values - high).astype(jnp.bfloat16)


def moments_after(clipped, first, second):
    return 0.9 * first + 0.1 * clipped, 0.95 * second + 0.05 * clipped * clipped


def copied_kernel(tp, rows, direction_ref, factor_ref, old_ref, o_ref):
    wide = old_ref.shape[0]
    own = rows // tp
    held = wide // rows * own
    at = lax.broadcasted_iota(jnp.int32, (wide, wide), 0)
    source = lax.broadcasted_iota(jnp.int32, (wide, wide), 1)
    wanted = at % rows // own * held + at // rows * own + at % own
    turn = jnp.where(source == wanted, 1.0, 0.0).astype(jnp.bfloat16)
    stacked = direction_ref[...].reshape(wide, RANK)
    direction = jnp.dot(turn, stacked, preferred_element_type=jnp.float32)
    update = lax.dot_general(
        direction.astype(jnp.bfloat16),
        factor_ref[...],
        (((1,), (1,)), ((), ())),
        preferred_element_type=jnp.float32,
    )
    o_ref[...] = (old_ref[...] - 0.05 * update).astype(jnp.bfloat16)


def copied_weight(directions, factor, old, fs, tp):
    hv, width = old.shape
    rows = hv // fs
    wide = 256
    held = wide // tp
    return pl.pallas_call(
        lambda *refs: copied_kernel(tp, rows, *refs),
        grid=(hv // wide,),
        in_specs=[
            pl.BlockSpec((tp, held, RANK), lambda k: (0, k, 0)),
            pl.BlockSpec((width, RANK), lambda k: (0, 0)),
            pl.BlockSpec((wide, width), lambda k: (k, 0)),
        ],
        out_specs=pl.BlockSpec((wide, width), lambda k: (k, 0)),
        out_shape=jax.ShapeDtypeStruct((hv, width), jnp.bfloat16),
        name="copied_weight",
    )(directions, factor, old)


def on_device(saved_input, out_cotangent, old_weight, factor, moment_first, moment_second):
    fs, tp = lax.axis_size(FS), lax.axis_size("tp")
    rows = HV // fs
    mine = rows // tp
    all_old = lax.all_gather(old_weight, FS, axis=0, tiled=True)
    contract = (((0,), (0,)), ((), ()))
    low = jnp.dot(out_cotangent, factor, preferred_element_type=jnp.float32)
    part = lax.dot_general(
        saved_input, low.astype(jnp.bfloat16), contract, preferred_element_type=jnp.float32
    )
    part = part.astype(jnp.bfloat16).reshape(fs, tp, mine, RANK).transpose(1, 0, 2, 3)
    tiles = exchanged(part.reshape(tp, fs * mine, RANK), "tp")
    part = jnp.sum(tiles.astype(jnp.float32), axis=0).reshape(fs, mine, RANK)
    own = jnp.sum(exchanged(part, FS), axis=0)

    start = lax.axis_index("tp") * mine
    own_first = lax.dynamic_slice(moment_first, (start, 0), (mine, RANK))
    own_second = lax.dynamic_slice(moment_second, (start, 0), (mine, RANK))
    sent = jnp.concatenate(
        [own.astype(jnp.bfloat16), *in_two(own_first), own_second.astype(jnp.bfloat16)]
    )
    held = copy_for_each(sent, FS).astype(jnp.float32)
    held = [held[:, k * mine : (k + 1) * mine] for k in range(4)]
    squares = jnp.full((1, RANK), jnp.sum(held[0] * held[0]), jnp.float32)
    sent = jnp.concatenate([own, squares, jnp.zeros((7 - mine, RANK), jnp.float32)])
    tiles = copy_for_each(sent, "tp")
    clip = jnp.minimum(1.0, LIMIT / (jnp.sqrt(jnp.sum(tiles[:, mine, 0])) + 1e-06))
    first, second = moments_after(clip * held[0], held[1] + held[2], held[3])
    directions = (first / (jnp.sqrt(second) + 1e-08)).astype(jnp.bfloat16)
    directions = copy_for_each(directions.reshape(fs * mine, RANK), "tp")

    projected = tiles[:, :mine].reshape(rows, RANK)
    new_first, new_second = moments_after(clip * projected, moment_first, moment_second)
    direction = new_first / (jnp.sqrt(new_second) + 1e-08)
    update = jnp.dot(direction, factor.astype(jnp.float32).T, precision=lax.Precision.HIGHEST)
    new_weight = old_weight - 0.05 * update
    copied = copied_weight(directions, factor, all_old, fs, tp)
    return (new_weight, update, new_first, new_second, copied)


def solution(mesh):
    finer = Mesh(mesh.devices.reshape(8, 8, mesh.shape["tp"]), (*FS, "tp"))
    in_specs = (P(FS, None), P(FS, "tp"), P(FS, "tp"), P("tp", None), P(FS, None), P(FS, None))
    out_specs = (P(FS, "tp"), P(FS, "tp"), P(FS, None), P(FS, None), P(None, "tp"))
    return jax.shard_map(
        on_device, mesh=finer, in_specs=in_specs, out_specs=out_specs, check_vma=False
    )
```

profile of v0, /device:TPU:1, one launch (start us, length us, event | category | flops | bytes accessed | tf_op | source)
XLA Modules:
  0.0 142.7 jit_solution(17214721601285085150)
XLA Ops:
  7.2 0.0 copy-start
  7.2 0.0 all-gather.2.cloned.1.call-start
  7.2 0.7 all-gather.2.cloned.1.call-update
  7.9 0.5 copy-done
  8.4 4.4 %fusion = bf16[2048,256]{0,1:T(8,128)(2,1)S(1)} fusion(bf16[1024,2048]{1,0:T(8,128)(2,1)} %param.6, bf16[1024,512]{1,0:T(8,128)(2,1)S(1)} %copy-done, bf16[512,256]{1,0:T(8,128)(2,1)} %refs_1_.1), kind=kOutput, calls=%fused_computation.1 | convolution fusion | flops 1342963712 | bytes 6553600 | tf_op jit(solution)/shard_map/dot_general | solution.py:79
  12.8 0.5 copy.19
  13.3 0.3 reshape.25
  13.6 0.2 copy.20
  13.8 0.2 copy.21
  14.1 24.2 %all_to_all.25 = bf16[8,256,256]{2,1,0:T(8,128)(2,1)S(1)} all-to-all(bf16[8,256,256]{2,1,0:T(8,128)(2,1)S(1)} %copy.21), channel_id=1, replica_groups=mesh['fs_0'=8,'fs_1'=8,'tp'=8] {'tp'}, dimensions={0} | all-to-all | bytes 2097152 | tf_op jit(solution)/shard_map/all_to_all | solution.py:17
  38.2 0.1 convert_reduce_fusion
  38.4 0.8 reshape.27
  39.2 12.7 %all-to-all-start.1 = ((f32[64,4,256]{2,1,0:T(4,128)}), f32[64,4,256]{2,1,0:T(4,128)S(1)}, u32[]{:S(2)}, u32[]{:S(2)}) async-start(f32[64,4,256]{2,1,0:T(4,128)} %reshape.27), calls=%async_computation.1 | async-start | bytes 524288 | tf_op jit(solution)/shard_map/all_to_all | solution.py:17
  51.9 12.3 %all-to-all-done.1 = f32[64,4,256]{2,1,0:T(4,128)S(1)} async-done(((f32[64,4,256]{2,1,0:T(4,128)}), f32[64,4,256]{2,1,0:T(4,128)S(1)}, u32[]{:S(2)}, u32[]{:S(2)}) %all-to-all-start.1) | async-done | bytes 262176 | tf_op jit(solution)/shard_map/all_to_all | solution.py:17
  64.2 0.1 reduce_sum.37
  64.3 0.8 broadcast_in_dim.12
  65.1 6.6 %all-to-all-start.2 = ((bf16[64,16,256]{2,1,0:T(8,128)(2,1)}), bf16[64,16,256]{2,1,0:T(8,128)(2,1)S(1)}, u32[]{:S(2)}, u32[]{:S(2)}) async-start(bf16[64,16,256]{2,1,0:T(8,128)(2,1)} %broadcast_in_dim.12), calls=%async_computation.2 | async-start | bytes 1048576 | tf_op jit(solution)/shard_map/all_to_all | solution.py:17
  71.8 0.1 pad.2.clone
  71.9 19.0 %all-to-all-done.2 = bf16[64,16,256]{2,1,0:T(8,128)(2,1)S(1)} async-done(((bf16[64,16,256]{2,1,0:T(8,128)(2,1)}), bf16[64,16,256]{2,1,0:T(8,128)(2,1)S(1)}, u32[]{:S(2)}, u32[]{:S(2)}) %all-to-all-start.2) | async-done | bytes 524320 | tf_op jit(solution)/shard_map/all_to_all | solution.py:17
  90.9 0.1 convert_element_type.39
  91.0 0.7 multiply_reduce_fusion
  91.8 0.7 pad.1.clone
  92.5 0.1 maximum_maximum_fusion
  92.6 12.6 %all_to_all.26 = f32[8,8,256]{2,1,0:T(8,128)S(1)} all-to-all(f32[8,8,256]{2,1,0:T(8,128)S(1)} %broadcast_in_dim.28), channel_id=1, replica_groups=mesh['fs_0'=8,'fs_1'=8,'tp'=8] {'tp'}, dimensions={0} | all-to-all | bytes 131072 | tf_op jit(solution)/shard_map/all_to_all | solution.py:17
  105.2 0.6 slice_reduce_fusion
  106.5 0.4 fusion.7
  107.0 1.0 broadcast_in_dim.30
  108.0 4.2 %all-to-all-start.4 = ((bf16[8,256,256]{2,1,0:T(8,128)(2,1)}), bf16[8,256,256]{2,1,0:T(8,128)(2,1)S(1)}, u32[]{:S(2)}, u32[]{:S(2)}) async-start(bf16[8,256,256]{2,1,0:T(8,128)(2,1)} %broadcast_in_dim.30), calls=%async_computation.4 | async-start | bytes 2097152 | tf_op jit(solution)/shard_map/all_to_all | solution.py:17
  112.3 1.0 multiply_subtract_fusion
  113.3 13.9 %all-to-all-done.4.refs_0_ = bf16[8,256,256]{2,1,0:T(8,128)(2,1)S(1)} async-done(((bf16[8,256,256]{2,1,0:T(8,128)(2,1)}), bf16[8,256,256]{2,1,0:T(8,128)(2,1)S(1)}, u32[]{:S(2)}, u32[]{:S(2)}) %all-to-all-start.4) | async-done | bytes 1048608 | tf_op jit(solution)/shard_map/all_to_all | solution.py:17
  127.2 1.0 copy-done.1
  128.2 7.7 %copied_weight.1 = bf16[2048,512]{1,0:T(8,128)(2,1)} custom-call(bf16[8,256,256]{2,1,0:T(8,128)(2,1)} %copy-done.1, bf16[512,256]{1,0:T(8,128)(2,1)} %refs_1_.1, f32[2048,512]{1,0:T(8,128)} %all-gather.2.cloned.1.call-done.refs_2_), custom_call_target="tpu_custom_call" | custom-call | tf_op jit(solution)/shard_map/copied_weight/pallas_call | solution.py:58
  (24 shorter events, 0.2 us)
Async XLA Ops:
  7.2 1.2 copy-start
  7.2 120.0 %all-gather.2.cloned.1.call-start = ((), (), s32[]{:S(2)}) async-start(), calls=%async_computation.5 | async-start | bytes 4259840 | tf_op jit(solution)/shard_map/all_gather | solution.py:76
  13.6 38.2 %copy-start.7 = (f32[32,256]{1,0:T(8,128)S(1)}, f32[32,256]{1,0:T(8,128)}, u32[]{:S(2)}) copy-start(f32[32,256]{1,0:T(8,128)} %param.11) | copy-start | bytes 98308
  13.6 38.3 %copy-start.6 = (f32[32,256]{1,0:T(8,128)S(1)}, f32[32,256]{1,0:T(8,128)}, u32[]{:S(2)}) copy-start(f32[32,256]{1,0:T(8,128)} %param.10) | copy-start | bytes 98308
  39.2 25.0 %all-to-all-start.1 = ((f32[64,4,256]{2,1,0:T(4,128)}), f32[64,4,256]{2,1,0:T(4,128)S(1)}, u32[]{:S(2)}, u32[]{:S(2)}) async-start(f32[64,4,256]{2,1,0:T(4,128)} %reshape.27), calls=%async_computation.1 | async-start | bytes 524288 | tf_op jit(solution)/shard_map/all_to_all | solution.py:17
  65.1 47.2 %copy-start.2 = (bf16[512,256]{1,0:T(8,128)(2,1)S(1)}, bf16[512,256]{1,0:T(8,128)(2,1)}, u32[]{:S(2)}) copy-start(bf16[512,256]{1,0:T(8,128)(2,1)} %refs_1_.1) | copy-start | bytes 786436
  65.1 47.2 %copy-start.3 = (f32[32,512]{1,0:T(8,128)S(1)}, f32[32,512]{1,0:T(8,128)}, u32[]{:S(2)}) copy-start(f32[32,512]{1,0:T(8,128)} %param.8) | copy-start | bytes 196612
  65.1 25.8 %all-to-all-start.2 = ((bf16[64,16,256]{2,1,0:T(8,128)(2,1)}), bf16[64,16,256]{2,1,0:T(8,128)(2,1)S(1)}, u32[]{:S(2)}, u32[]{:S(2)}) async-start(bf16[64,16,256]{2,1,0:T(8,128)(2,1)} %broadcast_in_dim.12), calls=%async_computation.2 | async-start | bytes 1048576 | tf_op jit(solution)/shard_map/all_to_all | solution.py:17
  108.0 19.2 %all-to-all-start.4 = ((bf16[8,256,256]{2,1,0:T(8,128)(2,1)}), bf16[8,256,256]{2,1,0:T(8,128)(2,1)S(1)}, u32[]{:S(2)}, u32[]{:S(2)}) async-start(bf16[8,256,256]{2,1,0:T(8,128)(2,1)} %broadcast_in_dim.30), calls=%async_computation.4 | async-start | bytes 2097152 | tf_op jit(solution)/shard_map/all_to_all | solution.py:17
  112.3 23.6 %copy-start.4 = (f32[32,256]{1,0:T(8,128)}, f32[32,256]{1,0:T(8,128)S(1)}, u32[]{:S(2)}) copy-start(f32[32,256]{1,0:T(8,128)S(1)} %get-tuple-element.5) | copy-start | bytes 98308
  112.3 23.6 %copy-start.5 = (f32[32,256]{1,0:T(8,128)}, f32[32,256]{1,0:T(8,128)S(1)}, u32[]{:S(2)}) copy-start(f32[32,256]{1,0:T(8,128)S(1)} %get-tuple-element.6) | copy-start | bytes 98308
  127.2 1.0 copy-start.1
Sparse Core Ops, SparseCore 0:
  11.1 99.2 all-gather.1
where the time goes:
time: 143 us
  waiting for transfers between devices  45.9 us (32%)
  blocking collectives  36.8 us (26%)
  starting transfers between devices  23.5 us (16%)
  between operations  15 us (10%)
  Pallas kernels  7.68 us (5%)
  local copies, waits for them, and re-layouts  6.24 us (4%)
  matrix products  5.34 us (4%)
  other arithmetic  2.25 us (2%)
    all_to_all x3, waiting for transfers between devices, exchanged(): return lax.all_to_all(blocks, axis, 0, 0, tiled=True)  45.2 us
    all_to_all x2, blocking collectives, exchanged(): return lax.all_to_all(blocks, axis, 0, 0, tiled=True)  36.8 us
    all_to_all x3, starting transfers between devices, exchanged(): return lax.all_to_all(blocks, axis, 0, 0, tiled=True)  23.5 us
    pallas_call x1, Pallas kernels, copied_weight(): pl.pallas_call(lambda *refs: copied_kernel(tp, rows, *refs), grid=(hv //...  7.68 us
    dot_general x1, matrix products, on_device(): lax.dot_general(saved_input, low.astype(jnp.bfloat16), contract, preferre...  4.35 us
  transfers between devices with their start and end apart: 4, of which 3 were waited for; matrix products, arithmetic and copies ran while one was open for 9% of the time, Pallas kernels for 0%

commit v1 on v0

v1 whole, which is shorter than its diff:
```python
import math

import jax
import jax.numpy as jnp
from jax import lax
from jax.sharding import Mesh
from jax.sharding import PartitionSpec as P

HV = 2048
RANK = 256
FS = ("fs_0", "fs_1")
LIMIT = math.sqrt(HV * RANK)


def exchanged(blocks, axis):
    return lax.all_to_all(blocks, axis, 0, 0, tiled=True)


def copy_for_each(shard, axis):
    devices = lax.axis_size(axis)
    return exchanged(jnp.broadcast_to(shard[None], (devices, *shard.shape)), axis)


def in_two(values):
    high = lax.reduce_precision(values, 8, 7)
    return high.astype(jnp.bfloat16), (values - high).astype(jnp.bfloat16)


def moments_after(clipped, first, second):
    return 0.9 * first + 0.1 * clipped, 0.95 * second + 0.05 * clipped * clipped


def on_device(saved_input, out_cotangent, old_weight, factor, moment_first, moment_second):
    fs, tp = lax.axis_size(FS), lax.axis_size("tp")
    rows = HV // fs
    mine = rows // tp
    all_old = lax.all_gather(old_weight, FS, axis=0, tiled=True)
    contract = (((0,), (0,)), ((), ()))
    low = jnp.dot(out_cotangent, factor, preferred_element_type=jnp.float32)
    part = lax.dot_general(
        saved_input, low.astype(jnp.bfloat16), contract, preferred_element_type=jnp.float32
    )
    part = part.astype(jnp.bfloat16).reshape(fs, tp, mine, RANK).transpose(1, 0, 2, 3)
    start = lax.axis_index("tp") * mine
    own_first = lax.dynamic_slice(moment_first, (start, 0), (mine, RANK))
    own_second = lax.dynamic_slice(moment_second, (start, 0), (mine, RANK))
    moments = jnp.concatenate([*in_two(own_first), own_second.astype(jnp.bfloat16)])
    part, moments = lax.optimization_barrier((part.reshape(tp, fs * mine, RANK), moments))
    tiles = exchanged(part, "tp")
    part = jnp.sum(tiles.astype(jnp.float32), axis=0).astype(jnp.bfloat16)
    tiles = exchanged(part.reshape(fs, mine, RANK), FS)
    own = jnp.sum(tiles.astype(jnp.float32), axis=0)

    held = copy_for_each(jnp.concatenate([own.astype(jnp.bfloat16), moments]), FS)
    held = lax.optimization_barrier(held.astype(jnp.float32))
    held = [held[:, k * mine : (k + 1) * mine] for k in range(4)]
    squares = jnp.sum(held[0] * held[0], axis=(0, 1))[None]
    sent = jnp.concatenate([own, jnp.broadcast_to(squares, (8 - mine, RANK))])
    tiles = copy_for_each(sent, "tp")
    squares = jnp.sum(tiles[:, mine], axis=0, keepdims=True)
    ones = jnp.ones((RANK, RANK), jnp.float32)
    squares = jnp.dot(squares, ones, precision=lax.Precision.HIGHEST)
    clip = jnp.minimum(1.0, LIMIT / (jnp.sqrt(squares) + 1e-06))
    first, second = moments_after(clip * held[0], held[1] + held[2], held[3])
    directions = (first / (jnp.sqrt(second) + 1e-08)).astype(jnp.bfloat16)
    directions = copy_for_each(directions.reshape(fs * mine, RANK), "tp")

    directions, tiles, clip = lax.optimization_barrier((directions, tiles, clip))
    directions = directions.reshape(tp, fs, mine, RANK).transpose(1, 0, 2, 3).reshape(HV, RANK)
    copied = lax.dot_general(
        directions, factor, (((1,), (1,)), ((), ())), preferred_element_type=jnp.float32
    )
    copied = (all_old - 0.05 * copied).astype(jnp.bfloat16)
    projected = tiles[:, :mine].reshape(rows, RANK)
    new_first, new_second = moments_after(clip * projected, moment_first, moment_second)
    direction = new_first / (jnp.sqrt(new_second) + 1e-08)
    update = jnp.dot(direction, factor.astype(jnp.float32).T, precision=lax.Precision.HIGHEST)
    new_weight = old_weight - 0.05 * update
    return (new_weight, update, new_first, new_second, copied)


def solution(mesh):
    finer = Mesh(mesh.devices.reshape(8, 8, mesh.shape["tp"]), (*FS, "tp"))
    in_specs = (P(FS, None), P(FS, "tp"), P(FS, "tp"), P("tp", None), P(FS, None), P(FS, None))
    out_specs = (P(FS, "tp"), P(FS, "tp"), P(FS, None), P(FS, None), P(None, "tp"))
    return jax.shard_map(
        on_device, mesh=finer, in_specs=in_specs, out_specs=out_specs, check_vma=False
    )
```

time: 143 us -> 133 us (0.930)
  blocking collectives: 36.8 us -> 101 us
  waiting for transfers between devices: 45.9 us -> 0.68 us
  starting transfers between devices: 23.5 us -> 0.04 us
  Pallas kernels: 7.68 us -> 0 us
  matrix products: 5.34 us -> 9.83 us
  local copies, waits for them, and re-layouts: 6.24 us -> 4.08 us
    all_to_all x2 -> x5, blocking collectives: 36.8 us -> 101 us  [exchanged(): return lax.all_to_all(blocks, axis, 0, 0, tiled=True)]
    all_to_all x3 -> x0, waiting for transfers between devices: 45.2 us -> none  [exchanged(): return lax.all_to_all(blocks, axis, 0, 0, tiled=True)]
    all_to_all x3 -> x0, starting transfers between devices: 23.5 us -> none  [exchanged(): return lax.all_to_all(blocks, axis, 0, 0, tiled=True)]
    pallas_call x1 -> x0, Pallas kernels: 7.68 us -> none  [copied_weight(): pl.pallas_call(lambda *refs: copied_kernel(tp, rows, *refs), grid=(hv //...]
    dot_general x0 -> x2, matrix products: none -> 4.48 us  [the longest x1 4.32 us: on_device(): lax.dot_general(directions, factor, (((1,), (1,)), ((), ())), preferred_e...]
    broadcast_in_dim x4, local copies, waits for them, and re-layouts: 1.91 us -> 0.15 us  [copy_for_each(): jnp.broadcast_to(shard[None], (devices, *shard.shape))]
  transfers between devices with their start and end apart: 4 -> 1, of which waited for: 3 -> 0; matrix products, arithmetic and copies ran while one was open for 9% -> 9% of each run, Pallas kernels for 0% -> 0%
where the time goes in v1:
time: 133 us; the launch traced here: 132 us
  blocking collectives  101 us (76%)
  between operations  14.2 us (11%)
  matrix products  9.83 us (7%)
  local copies, waits for them, and re-layouts  4.08 us (3%)
  other arithmetic  2.42 us (2%)
    all_to_all x5, blocking collectives, exchanged(): return lax.all_to_all(blocks, axis, 0, 0, tiled=True)  101 us
    dot_general x1, matrix products, on_device(): lax.dot_general(saved_input, low.astype(jnp.bfloat16), contract, preferre...  4.35 us
    dot_general x1, matrix products, on_device(): lax.dot_general(directions, factor, (((1,), (1,)), ((), ())), preferred_e...  4.32 us
  transfers between devices with their start and end apart: 1, of which 0 were waited for; matrix products, arithmetic and copies ran while one was open for 9% of the time, Pallas kernels for 0%

profile of v1, /device:TPU:1, one launch (start us, length us, event | category | flops | bytes accessed | tf_op | source)
XLA Modules:
  0.0 132.3 jit_solution(14801160072825833063)
XLA Ops:
  7.2 0.0 copy-start
  7.2 0.0 all-gather.2.cloned.1.call-start
  7.2 0.7 all-gather.2.cloned.1.call-update
  7.9 0.5 copy-done
  8.4 4.4 %fusion = bf16[2048,256]{0,1:T(8,128)(2,1)S(1)} fusion(bf16[1024,2048]{1,0:T(8,128)(2,1)} %param.6, bf16[1024,512]{1,0:T(8,128)(2,1)S(1)} %copy-done, bf16[512,256]{1,0:T(8,128)(2,1)} %param.9), kind=kOutput, calls=%fused_computation.2 | convolution fusion | flops 1342963712 | bytes 6553600 | tf_op jit(solution)/shard_map/dot_general | solution.py:40
  12.8 0.5 copy.38
  13.3 0.3 reshape.41
  13.6 0.2 copy.39
  13.8 0.7 dynamic-slice_convert_fusion
  14.5 0.7 reduce-precision_convert_fusion
  15.2 0.2 copy.40
  15.5 24.2 %all_to_all.25 = bf16[8,256,256]{2,1,0:T(8,128)(2,1)S(1)} all-to-all(bf16[8,256,256]{2,1,0:T(8,128)(2,1)S(1)} %copy.40), channel_id=1, replica_groups=mesh['fs_0'=8,'fs_1'=8,'tp'=8] {'tp'}, dimensions={0} | all-to-all | bytes 2097152 | tf_op jit(solution)/shard_map/all_to_all | solution.py:16
  39.6 0.1 reduce_sum.39
  39.8 23.9 %all_to_all.26 = bf16[64,4,256]{2,1,0:T(4,128)(2,1)S(1)} all-to-all(bf16[64,4,256]{2,1,0:T(4,128)(2,1)S(1)} %reshape.43), channel_id=1, replica_groups=mesh['fs_0'=8,'fs_1'=8,'tp'=8] {'fs_0','fs_1'}, dimensions={0} | all-to-all | bytes 262144 | tf_op jit(solution)/shard_map/all_to_all | solution.py:16
  63.8 19.9 %all_to_all.27 = bf16[64,16,256]{2,1,0:T(8,128)(2,1)S(1)} all-to-all(bf16[64,16,256]{2,1,0:T(8,128)(2,1)S(1)} %broadcast_in_dim.12), channel_id=1, replica_groups=mesh['fs_0'=8,'fs_1'=8,'tp'=8] {'fs_0','fs_1'}, dimensions={0} | all-to-all | bytes 1048576 | tf_op jit(solution)/shard_map/all_to_all | solution.py:16
  83.7 0.1 convert_element_type.44
  83.8 0.1 multiply_reduce_fusion
  83.9 14.9 %all_to_all.28 = f32[8,8,256]{2,1,0:T(8,128)S(1)} all-to-all(f32[8,8,256]{2,1,0:T(8,128)S(1)} %broadcast_in_dim.14), channel_id=1, replica_groups=mesh['fs_0'=8,'fs_1'=8,'tp'=8] {'tp'}, dimensions={0} | all-to-all | bytes 131072 | tf_op jit(solution)/shard_map/all_to_all | solution.py:16
  98.9 0.2 fusion.8
  99.1 0.4 fusion.7
  99.5 0.1 broadcast_in_dim.17
  99.6 0.0 copy-start.1
  99.6 0.0 copy-start.2
  99.6 18.2 %all_to_all.29 = bf16[8,256,256]{2,1,0:T(8,128)(2,1)S(1)} all-to-all(bf16[8,256,256]{2,1,0:T(8,128)(2,1)S(1)} %broadcast_in_dim.17), channel_id=1, replica_groups=mesh['fs_0'=8,'fs_1'=8,'tp'=8] {'tp'}, dimensions={0} | all-to-all | bytes 2097152 | tf_op jit(solution)/shard_map/all_to_all | solution.py:16
  117.8 0.6 copy.42
  118.4 0.5 copy.43
  119.0 0.3 reshape.46
  119.3 0.8 fusion.10
  120.1 0.0 copy-start.3
  120.1 0.0 copy-start.4
  120.1 1.0 multiply_subtract_fusion
  121.1 4.3 %subtract_convert_fusion = bf16[2048,512]{1,0:T(8,128)(2,1)} fusion(f32[2048,512]{1,0:T(8,128)} %all-gather.2.cloned.1.call-done, bf16[2048,256]{1,0:T(8,128)(2,1)S(1)} %reshape.46, bf16[512,256]{1,0:T(8,128)(2,1)S(1)} %copy-done.1), kind=kOutput, calls=%fused_computation | convolution fusion | flops 540016640 | bytes 7602176 | tf_op jit(solution)/shard_map/dot_general | solution.py:70
  (19 shorter events, 0.3 us)
Async XLA Ops:
  7.2 1.2 copy-start
  7.2 114.0 %all-gather.2.cloned.1.call-start = ((), (), s32[]{:S(2)}) async-start(), calls=%async_computation.5 | async-start | bytes 4259840 | tf_op jit(solution)/shard_map/all_gather | solution.py:37
  99.6 20.5 %copy-start.1 = (bf16[512,256]{1,0:T(8,128)(2,1)S(1)}, bf16[512,256]{1,0:T(8,128)(2,1)}, u32[]{:S(2)}) copy-start(bf16[512,256]{1,0:T(8,128)(2,1)} %param.9) | copy-start | bytes 786436
  99.6 20.5 %copy-start.2 = (f32[32,512]{1,0:T(8,128)S(1)}, f32[32,512]{1,0:T(8,128)}, u32[]{:S(2)}) copy-start(f32[32,512]{1,0:T(8,128)} %param.8) | copy-start | bytes 196612
  120.1 5.4 %copy-start.3 = (f32[32,256]{1,0:T(8,128)}, f32[32,256]{1,0:T(8,128)S(1)}, u32[]{:S(2)}) copy-start(f32[32,256]{1,0:T(8,128)S(1)} %get-tuple-element.15) | copy-start | bytes 98308
  120.1 5.3 %copy-start.4 = (f32[32,256]{1,0:T(8,128)}, f32[32,256]{1,0:T(8,128)S(1)}, u32[]{:S(2)}) copy-start(f32[32,256]{1,0:T(8,128)S(1)} %get-tuple-element.16) | copy-start | bytes 98308
Sparse Core Ops, SparseCore 0:
  11.1 95.2 all-gather.1

commit v2 on v1

v2 whole, which is shorter than its diff:
```python
import math

import jax
import jax.numpy as jnp
from jax import lax
from jax.sharding import Mesh
from jax.sharding import PartitionSpec as P

HV = 2048
RANK = 256
FS = ("fs_0", "fs_1")
TP = ("tp_0", "tp_1")
LIMIT = math.sqrt(HV * RANK)


def exchanged(blocks, axis):
    return lax.all_to_all(blocks, axis, 0, 0, tiled=True)


def copy_for_each(shard, axis):
    devices = lax.axis_size(axis)
    return exchanged(jnp.broadcast_to(shard[None], (devices, *shard.shape)), axis)


def in_two(values):
    high = lax.reduce_precision(values, 8, 7)
    return high.astype(jnp.bfloat16), (values - high).astype(jnp.bfloat16)


def moments_after(clipped, first, second):
    return 0.9 * first + 0.1 * clipped, 0.95 * second + 0.05 * clipped * clipped


def on_device(saved_input, out_cotangent, old_weight, factor, moment_first, moment_second):
    fs, tp = lax.axis_size(FS), lax.axis_size(TP)
    rows = HV // fs
    mine = rows // tp
    all_old = lax.all_gather(old_weight, FS, axis=0, tiled=True)
    contract = (((0,), (0,)), ((), ()))
    low = jnp.dot(out_cotangent, factor, preferred_element_type=jnp.float32)
    part = lax.dot_general(
        saved_input, low.astype(jnp.bfloat16), contract, preferred_element_type=jnp.float32
    )
    part = part.astype(jnp.bfloat16).reshape(fs, tp, mine, RANK).transpose(1, 0, 2, 3)
    start = (lax.axis_index(TP) * mine).astype(jnp.uint32)
    part, start = lax.optimization_barrier((part.reshape(tp, fs * mine, RANK), start))
    tiles = exchanged(part, TP)
    part = jnp.sum(tiles.astype(jnp.float32), axis=0).astype(jnp.bfloat16)
    tiles = exchanged(part.reshape(fs, mine, RANK), FS)
    own = jnp.sum(tiles.astype(jnp.float32), axis=0)

    own, first, second = lax.optimization_barrier((own, moment_first, moment_second))
    own_first = lax.dynamic_slice(first, (start, jnp.uint32(0)), (mine, RANK))
    own_second = lax.dynamic_slice(second, (start, jnp.uint32(0)), (mine, RANK))
    moments = [*in_two(own_first), own_second.astype(jnp.bfloat16)]
    held = copy_for_each(jnp.concatenate([own.astype(jnp.bfloat16), *moments]), FS)
    held = lax.optimization_barrier(held.astype(jnp.float32))
    held = [held[:, k * mine : (k + 1) * mine] for k in range(4)]
    squares = jnp.sum(held[0] * held[0], axis=(0, 1))[None]
    sent = jnp.concatenate([own, jnp.broadcast_to(squares, (8 - mine, RANK))])
    tiles = copy_for_each(sent, TP)
    squares = jnp.sum(tiles[:, mine], axis=0, keepdims=True)
    ones = jnp.ones((RANK, RANK), jnp.float32)
    squares = jnp.dot(squares, ones, precision=lax.Precision.HIGHEST)
    clip = jnp.minimum(1.0, LIMIT / (jnp.sqrt(squares) + 1e-06))
    all_first, all_second = moments_after(clip * held[0], held[1] + held[2], held[3])
    directions = (all_first / (jnp.sqrt(all_second) + 1e-08)).astype(jnp.bfloat16)
    directions = copy_for_each(directions.reshape(fs * mine, RANK), TP[0])
    directions, all_old = lax.optimization_barrier((directions, all_old))
    directions = copy_for_each(directions.reshape(-1, RANK), TP[1])

    directions, tiles, clip = lax.optimization_barrier((directions, tiles, clip))
    projected = tiles[:, :mine].reshape(rows, RANK)
    new_first, new_second = moments_after(clip * projected, first, second)
    direction = new_first / (jnp.sqrt(new_second) + 1e-08)
    update = jnp.dot(direction, factor.astype(jnp.float32).T, precision=lax.Precision.HIGHEST)
    new_weight = old_weight - 0.05 * update
    mine = (new_weight, update, new_first, new_second)
    directions, mine = lax.optimization_barrier((directions, mine))
    directions = directions.reshape(lax.axis_size(TP[1]), lax.axis_size(TP[0]), fs, rows // tp, RANK)
    directions = directions.transpose(2, 1, 0, 3, 4).reshape(HV, RANK)
    copied = lax.dot_general(
        directions, factor, (((1,), (1,)), ((), ())), preferred_element_type=jnp.float32
    )
    copied = (all_old - 0.05 * copied).astype(jnp.bfloat16)
    return (*mine, copied)


def solution(mesh):
    finer = Mesh(mesh.devices.reshape(8, 8, mesh.shape["tp"] // 2, 2), (*FS, *TP))
    in_specs = (P(FS, None), P(FS, TP), P(FS, TP), P(TP, None), P(FS, None), P(FS, None))
    out_specs = (P(FS, TP), P(FS, TP), P(FS, None), P(FS, None), P(None, TP))
    return jax.shard_map(
        on_device, mesh=finer, in_specs=in_specs, out_specs=out_specs, check_vma=False
    )
```

time: 133 us -> 129 us (0.970)
  blocking collectives: 101 us -> 99.3 us
  other arithmetic: 2.42 us -> 0.94 us
    all_to_all x5 -> x6, blocking collectives: 101 us -> 99.3 us  [exchanged(): return lax.all_to_all(blocks, axis, 0, 0, tiled=True)]
  transfers between devices with their start and end apart: 1 -> 1, of which waited for: 0 -> 0; matrix products, arithmetic and copies ran while one was open for 9% -> 5% of each run, Pallas kernels for 0% -> 0%
where the time goes in v2:
time: 129 us
  blocking collectives  99.3 us (77%)
  between operations  14.3 us (11%)
  matrix products  9.76 us (8%)
  local copies, waits for them, and re-layouts  3.97 us (3%)
    all_to_all x6, blocking collectives, exchanged(): return lax.all_to_all(blocks, axis, 0, 0, tiled=True)  99.3 us
    dot_general x1, matrix products, on_device(): lax.dot_general(saved_input, low.astype(jnp.bfloat16), contract, preferre...  4.35 us
    dot_general x1, matrix products, on_device(): lax.dot_general(directions, factor, (((1,), (1,)), ((), ())), preferred_e...  4.25 us
  transfers between devices with their start and end apart: 1, of which 0 were waited for; matrix products, arithmetic and copies ran while one was open for 5% of the time, Pallas kernels for 0%

profile of v2, /device:TPU:1, one launch (start us, length us, event | category | flops | bytes accessed | tf_op | source)
XLA Modules:
  0.0 129.0 jit_solution(17624732709691923738)
XLA Ops:
  7.2 0.0 copy-start
  7.2 0.0 all-gather.2.cloned.1.call-start
  7.2 0.7 all-gather.2.cloned.1.call-update
  7.9 0.5 copy-done
  8.4 4.4 %fusion = bf16[2048,256]{0,1:T(8,128)(2,1)S(1)} fusion(bf16[1024,2048]{1,0:T(8,128)(2,1)} %param.6, bf16[1024,512]{1,0:T(8,128)(2,1)S(1)} %copy-done, bf16[512,256]{1,0:T(8,128)(2,1)} %param.9), kind=kOutput, calls=%fused_computation.2 | convolution fusion | flops 1342963712 | bytes 6553600 | tf_op jit(solution)/shard_map/dot_general | solution.py:41
  12.8 0.5 copy.38
  13.3 0.3 reshape.42
  13.6 0.0 copy-start.6
  13.6 0.0 copy-start.5
  13.6 0.2 copy.39
  13.8 0.2 copy.40
  14.1 24.2 %all_to_all.30 = bf16[8,256,256]{2,1,0:T(8,128)(2,1)S(1)} all-to-all(bf16[8,256,256]{2,1,0:T(8,128)(2,1)S(1)} %copy.40), channel_id=1, replica_groups=mesh['fs_0'=8,'fs_1'=8,'tp_0'=4,'tp_1'=2] {'tp_0','tp_1'}, dimensions={0} | all-to-all | bytes 2097152 | tf_op jit(solution)/shard_map/all_to_all | solution.py:17
  38.2 0.1 reduce_sum.39
  38.4 24.1 %all_to_all.31 = bf16[64,4,256]{2,1,0:T(4,128)(2,1)S(1)} all-to-all(bf16[64,4,256]{2,1,0:T(4,128)(2,1)S(1)} %reshape.44), channel_id=1, replica_groups=mesh['fs_0'=8,'fs_1'=8,'tp_0'=4,'tp_1'=2] {'fs_0','fs_1'}, dimensions={0} | all-to-all | bytes 262144 | tf_op jit(solution)/shard_map/all_to_all | solution.py:17
  62.7 19.9 %all_to_all.32 = bf16[64,16,256]{2,1,0:T(8,128)(2,1)S(1)} all-to-all(bf16[64,16,256]{2,1,0:T(8,128)(2,1)S(1)} %broadcast_in_dim.16), channel_id=1, replica_groups=mesh['fs_0'=8,'fs_1'=8,'tp_0'=4,'tp_1'=2] {'fs_0','fs_1'}, dimensions={0} | all-to-all | bytes 1048576 | tf_op jit(solution)/shard_map/all_to_all | solution.py:17
  82.6 0.1 convert_element_type.48
  82.7 0.0 copy-start.1
  82.7 0.0 copy-start.2
  82.7 0.1 multiply_reduce_fusion
  82.9 14.1 %all_to_all.33 = f32[8,8,256]{2,1,0:T(8,128)S(1)} all-to-all(f32[8,8,256]{2,1,0:T(8,128)S(1)} %broadcast_in_dim.18), channel_id=1, replica_groups=mesh['fs_0'=8,'fs_1'=8,'tp_0'=4,'tp_1'=2] {'tp_0','tp_1'}, dimensions={0} | all-to-all | bytes 131072 | tf_op jit(solution)/shard_map/all_to_all | solution.py:17
  97.0 0.2 fusion.8
  97.2 0.4 fusion.7
  97.7 11.0 %all_to_all.34 = bf16[4,256,256]{2,1,0:T(8,128)(2,1)S(1)} all-to-all(bf16[4,256,256]{2,1,0:T(8,128)(2,1)S(1)} %broadcast_in_dim.42), channel_id=1, replica_groups=mesh['fs_0'=8,'fs_1'=8,'tp_0'=4,'tp_1'=2] {'tp_0'}, dimensions={0} | all-to-all | bytes 1048576 | tf_op jit(solution)/shard_map/all_to_all | solution.py:17
  108.8 0.1 broadcast_in_dim.44
  108.8 6.0 %all_to_all.35 = bf16[2,1024,256]{2,1,0:T(8,128)(2,1)S(1)} all-to-all(bf16[2,1024,256]{2,1,0:T(8,128)(2,1)S(1)} %broadcast_in_dim.44), channel_id=1, replica_groups=mesh['fs_0'=8,'fs_1'=8,'tp_0'=4,'tp_1'=2] {'tp_1'}, dimensions={0} | all-to-all | bytes 2097152 | tf_op jit(solution)/shard_map/all_to_all | solution.py:17
  114.9 0.0 copy-start.3
  114.9 0.0 copy-start.4
  114.9 1.0 multiply_subtract_fusion
  115.9 1.1 copy.42
  117.0 0.6 copy.43
  117.6 0.3 reshape.47
  117.9 4.3 %subtract_convert_fusion = bf16[2048,512]{1,0:T(8,128)(2,1)} fusion(f32[2048,512]{1,0:T(8,128)} %all-gather.2.cloned.1.call-done, bf16[2048,256]{1,0:T(8,128)(2,1)S(1)} %reshape.47, bf16[512,256]{1,0:T(8,128)(2,1)S(1)} %copy-done.1), kind=kOutput, calls=%fused_computation | convolution fusion | flops 540016640 | bytes 7602176 | tf_op jit(solution)/shard_map/dot_general | solution.py:82
  (24 shorter events, 0.4 us)
Async XLA Ops:
  7.2 1.2 copy-start
  7.2 101.6 %all-gather.2.cloned.1.call-start = ((), (), s32[]{:S(2)}) async-start(), calls=%async_computation.6 | async-start | bytes 4259840 | tf_op jit(solution)/shard_map/all_gather | solution.py:38
  13.6 49.0 %copy-start.6 = (f32[32,256]{1,0:T(8,128)S(1)}, f32[32,256]{1,0:T(8,128)}, u32[]{:S(2)}) copy-start(f32[32,256]{1,0:T(8,128)} %param.11) | copy-start | bytes 98308
  13.6 49.0 %copy-start.5 = (f32[32,256]{1,0:T(8,128)S(1)}, f32[32,256]{1,0:T(8,128)}, u32[]{:S(2)}) copy-start(f32[32,256]{1,0:T(8,128)} %param.10) | copy-start | bytes 98308
  82.7 32.2 %copy-start.1 = (bf16[512,256]{1,0:T(8,128)(2,1)S(1)}, bf16[512,256]{1,0:T(8,128)(2,1)}, u32[]{:S(2)}) copy-start(bf16[512,256]{1,0:T(8,128)(2,1)} %param.9) | copy-start | bytes 786436
  82.7 32.2 %copy-start.2 = (f32[32,512]{1,0:T(8,128)S(1)}, f32[32,512]{1,0:T(8,128)}, u32[]{:S(2)}) copy-start(f32[32,512]{1,0:T(8,128)} %param.8) | copy-start | bytes 196612
  114.9 7.3 %copy-start.3 = (f32[32,256]{1,0:T(8,128)}, f32[32,256]{1,0:T(8,128)S(1)}, u32[]{:S(2)}) copy-start(f32[32,256]{1,0:T(8,128)S(1)} %get-tuple-element.18) | copy-start | bytes 98308
  114.9 7.2 %copy-start.4 = (f32[32,256]{1,0:T(8,128)}, f32[32,256]{1,0:T(8,128)S(1)}, u32[]{:S(2)}) copy-start(f32[32,256]{1,0:T(8,128)S(1)} %get-tuple-element.17) | copy-start | bytes 98308
Sparse Core Ops, SparseCore 0:
  11.1 94.7 all-gather.1

commit v3 on v2

--- a/solution.py
+++ b/solution.py
@@ -2,7 +2,10 @@
 
 import jax
 import jax.numpy as jnp
+import numpy as np
 from jax import lax
+from jax.experimental import pallas as pl
+from jax.experimental.pallas import tpu as pltpu
 from jax.sharding import Mesh
 from jax.sharding import PartitionSpec as P
 
@@ -31,19 +34,60 @@
     return 0.9 * first + 0.1 * clipped, 0.95 * second + 0.05 * clipped * clipped
 
 
+def projection_kernel(held, x_ref, g_ref, f_ref, turn_ref, o_ref, low_ref):
+    @pl.when(pl.program_id(0) == 0)
+    def _():
+        low = lax.dot_general(
+            f_ref[...], g_ref[...], (((0,), (1,)), ((), ())), preferred_element_type=jnp.float32
+        )
+        high = low.astype(jnp.bfloat16)
+        low_ref[:RANK] = high
+        low_ref[RANK:] = (low - high.astype(jnp.float32)).astype(jnp.bfloat16)
+
+    both = jnp.dot(low_ref[...], x_ref[...], preferred_element_type=jnp.float32)
+    part = (both[:RANK] + both[RANK:]).astype(jnp.bfloat16)
+    wide = turn_ref.shape[0]
+    for k in range(part.shape[1] // wide):
+        turned = lax.dot_general(
+            turn_ref[...],
+            part[:, k * wide : (k + 1) * wide],
+            (((1,), (1,)), ((), ())),
+            preferred_element_type=jnp.float32,
+        )
+        turned = turned.astype(jnp.bfloat16).reshape(-1, held, RANK)
+        o_ref[:, k * held : (k + 1) * held] = turned
+
+
+def projected_part(saved_input, out_cotangent, factor, fs, tp):
+    tokens, wide = saved_input.shape
+    width = out_cotangent.shape[1]
+    step, turned = 1024, 256
+    order = np.arange(turned).reshape(turned * fs // wide, tp, -1).transpose(1, 0, 2).reshape(-1)
+    turn = jnp.asarray(np.eye(turned, dtype=np.float32)[order], jnp.bfloat16)
+    return pl.pallas_call(
+        lambda *refs: projection_kernel(turned // tp, *refs),
+        grid=(wide // step,),
+        in_specs=[
+            pl.BlockSpec((tokens, step), lambda k: (0, k)),
+            pl.BlockSpec((tokens, width), lambda k: (0, 0)),
+            pl.BlockSpec((width, RANK), lambda k: (0, 0)),
+            pl.BlockSpec((turned, turned), lambda k: (0, 0)),
+        ],
+        out_specs=pl.BlockSpec((tp, step // tp, RANK), lambda k: (0, k, 0)),
+        out_shape=jax.ShapeDtypeStruct((tp, wide // tp, RANK), jnp.bfloat16),
+        scratch_shapes=[pltpu.VMEM((2 * RANK, tokens), jnp.bfloat16)],
+        name="projection",
+    )(saved_input, out_cotangent, factor, turn)
+
+
 def on_device(saved_input, out_cotangent, old_weight, factor, moment_first, moment_second):
     fs, tp = lax.axis_size(FS), lax.axis_size(TP)
     rows = HV // fs
     mine = rows // tp
     all_old = lax.all_gather(old_weight, FS, axis=0, tiled=True)
-    contract = (((0,), (0,)), ((), ()))
-    low = jnp.dot(out_cotangent, factor, preferred_element_type=jnp.float32)
-    part = lax.dot_general(
-        saved_input, low.astype(jnp.bfloat16), contract, preferred_element_type=jnp.float32
-    )
-    part = part.astype(jnp.bfloat16).reshape(fs, tp, mine, RANK).transpose(1, 0, 2, 3)
+    part = projected_part(saved_input, out_cotangent, factor, fs, tp)
     start = (lax.axis_index(TP) * mine).astype(jnp.uint32)
-    part, start = lax.optimization_barrier((part.reshape(tp, fs * mine, RANK), start))
+    part, start = lax.optimization_barrier((part, start))
     tiles = exchanged(part, TP)
     part = jnp.sum(tiles.astype(jnp.float32), axis=0).astype(jnp.bfloat16)
     tiles = exchanged(part.reshape(fs, mine, RANK), FS)
@@ -65,9 +109,9 @@
     clip = jnp.minimum(1.0, LIMIT / (jnp.sqrt(squares) + 1e-06))
     all_first, all_second = moments_after(clip * held[0], held[1] + held[2], held[3])
     directions = (all_first / (jnp.sqrt(all_second) + 1e-08)).astype(jnp.bfloat16)
-    directions = copy_for_each(directions.reshape(fs * mine, RANK), TP[0])
+    directions = copy_for_each(directions, TP[0])
     directions, all_old = lax.optimization_barrier((directions, all_old))
-    directions = copy_for_each(directions.reshape(-1, RANK), TP[1])
+    directions = copy_for_each(directions, TP[1])
 
     directions, tiles, clip = lax.optimization_barrier((directions, tiles, clip))
     projected = tiles[:, :mine].reshape(rows, RANK)
@@ -77,7 +121,6 @@
     new_weight = old_weight - 0.05 * update
     mine = (new_weight, update, new_first, new_second)
     directions, mine = lax.optimization_barrier((directions, mine))
-    directions = directions.reshape(lax.axis_size(TP[1]), lax.axis_size(TP[0]), fs, rows // tp, RANK)
     directions = directions.transpose(2, 1, 0, 3, 4).reshape(HV, RANK)
     copied = lax.dot_general(
         directions, factor, (((1,), (1,)), ((), ())), preferred_element_type=jnp.float32

time: 129 us -> 129 us (level)
  Pallas kernels: 0 us -> 6.17 us
  matrix products: 9.76 us -> 5.41 us
  local copies, waits for them, and re-layouts: 3.97 us -> 1.62 us
    pallas_call x0 -> x1, Pallas kernels: none -> 6.17 us  [projected_part(): pl.pallas_call(lambda *refs: projection_kernel(turned // tp, *refs), grid...]
    dot_general x1 -> x0, matrix products: 4.35 us -> none  [on_device(): lax.dot_general(saved_input, low.astype(jnp.bfloat16), contract, preferre...]
  transfers between devices with their start and end apart: 1 -> 1, of which waited for: 0 -> 0; matrix products, arithmetic and copies ran while one was open for 5% -> 1% of each run, Pallas kernels for 0% -> 5%
where the time goes in v3:
time: 129 us
  blocking collectives  99.6 us (77%)
  between operations  14.2 us (11%)
  Pallas kernels  6.17 us (5%)
  matrix products  5.41 us (4%)
  local copies, waits for them, and re-layouts  1.62 us (1%)
    all_to_all x6, blocking collectives, exchanged(): return lax.all_to_all(blocks, axis, 0, 0, tiled=True)  99.6 us
    pallas_call x1, Pallas kernels, projected_part(): pl.pallas_call(lambda *refs: projection_kernel(turned // tp, *refs), grid...  6.17 us
    dot_general x1, matrix products, on_device(): lax.dot_general(directions, factor, (((1,), (1,)), ((), ())), preferred_e...  4.25 us
  transfers between devices with their start and end apart: 1, of which 0 were waited for; matrix products, arithmetic and copies ran while one was open for 1% of the time, Pallas kernels for 5%

profile of v3, /device:TPU:1, one launch (start us, length us, event | category | flops | bytes accessed | tf_op | source)
XLA Modules:
  0.0 128.7 jit_solution(2892227604937824357)
XLA Ops:
  7.2 0.0 all-gather.2.cloned.1.call-start
  7.2 0.7 all-gather.2.cloned.1.call-update
  7.9 0.0 copy-start.5
  7.9 0.0 copy-start.4
  7.9 6.2 %projection.1 = bf16[8,256,256]{2,1,0:T(8,128)(2,1)} custom-call(bf16[1024,2048]{1,0:T(8,128)(2,1)} %refs_0_.1, bf16[1024,512]{1,0:T(8,128)(2,1)} %refs_1_.1, bf16[512,256]{1,0:T(8,128)(2,1)} %refs_2_.1, bf16[256,256]{1,0:T(8,128)(2,1)} %constant.12.clone.refs_3_), custom_call_target="tpu_custom_call" | custom-call | tf_op jit(solution)/shard_map/projection/pallas_call | solution.py:67
  14.1 25.2 %all_to_all.30 = bf16[8,256,256]{2,1,0:T(8,128)(2,1)S(1)} all-to-all(bf16[8,256,256]{2,1,0:T(8,128)(2,1)} %projection.1), channel_id=1, replica_groups=mesh['fs_0'=8,'fs_1'=8,'tp_0'=4,'tp_1'=2] {'tp_0','tp_1'}, dimensions={0} | all-to-all | bytes 2097152 | tf_op jit(solution)/shard_map/all_to_all | solution.py:20
  39.3 0.1 reduce_sum.39
  39.5 23.2 %all_to_all.31 = bf16[64,4,256]{2,1,0:T(4,128)(2,1)S(1)} all-to-all(bf16[64,4,256]{2,1,0:T(4,128)(2,1)S(1)} %reshape.33), channel_id=1, replica_groups=mesh['fs_0'=8,'fs_1'=8,'tp_0'=4,'tp_1'=2] {'fs_0','fs_1'}, dimensions={0} | all-to-all | bytes 262144 | tf_op jit(solution)/shard_map/all_to_all | solution.py:20
  62.8 0.0 copy-done.5
  62.8 0.0 copy-done.4
  62.9 19.7 %all_to_all.32 = bf16[64,16,256]{2,1,0:T(8,128)(2,1)S(1)} all-to-all(bf16[64,16,256]{2,1,0:T(8,128)(2,1)S(1)} %broadcast_in_dim.12), channel_id=1, replica_groups=mesh['fs_0'=8,'fs_1'=8,'tp_0'=4,'tp_1'=2] {'fs_0','fs_1'}, dimensions={0} | all-to-all | bytes 1048576 | tf_op jit(solution)/shard_map/all_to_all | solution.py:20
  82.6 0.1 convert_element_type.36
  82.8 0.0 copy-start
  82.8 0.0 copy-start.1
  82.8 0.1 multiply_reduce_fusion
  82.9 14.4 %all_to_all.33 = f32[8,8,256]{2,1,0:T(8,128)S(1)} all-to-all(f32[8,8,256]{2,1,0:T(8,128)S(1)} %broadcast_in_dim.14), channel_id=1, replica_groups=mesh['fs_0'=8,'fs_1'=8,'tp_0'=4,'tp_1'=2] {'tp_0','tp_1'}, dimensions={0} | all-to-all | bytes 131072 | tf_op jit(solution)/shard_map/all_to_all | solution.py:20
  97.3 0.2 fusion.7
  97.5 0.4 fusion.6
  97.9 0.1 broadcast_in_dim.16
  98.1 11.0 %all_to_all.34 = bf16[4,64,4,256]{3,2,1,0:T(4,128)(2,1)S(1)} all-to-all(bf16[4,64,4,256]{3,2,1,0:T(4,128)(2,1)S(1)} %broadcast_in_dim.16), channel_id=1, replica_groups=mesh['fs_0'=8,'fs_1'=8,'tp_0'=4,'tp_1'=2] {'tp_0'}, dimensions={0} | all-to-all | bytes 1048576 | tf_op jit(solution)/shard_map/all_to_all | solution.py:20
  109.1 0.2 copy.23
  109.3 0.3 broadcast_in_dim.17
  109.6 6.0 %all_to_all.35 = bf16[2,4,64,4,256]{4,3,1,2,0:T(4,128)(2,1)S(1)} all-to-all(bf16[2,4,64,4,256]{4,3,1,2,0:T(4,128)(2,1)S(1)} %broadcast_in_dim.17), channel_id=1, replica_groups=mesh['fs_0'=8,'fs_1'=8,'tp_0'=4,'tp_1'=2] {'tp_1'}, dimensions={0} | all-to-all | bytes 2097152 | tf_op jit(solution)/shard_map/all_to_all | solution.py:20
  115.6 0.0 copy-start.2
  115.7 0.0 copy-start.3
  115.7 0.0 copy-done
  115.7 0.0 copy-done.1
  115.7 1.0 multiply_subtract_fusion
  116.7 0.6 copy.24
  117.3 0.3 reshape.35
  117.6 4.3 %subtract_convert_fusion = bf16[2048,512]{1,0:T(8,128)(2,1)} fusion(f32[2048,512]{1,0:T(8,128)} %all-gather.2.cloned.1.call-done, bf16[2048,256]{1,0:T(8,128)(2,1)S(1)} %reshape.35, bf16[512,256]{1,0:T(8,128)(2,1)S(1)} %copy-done), kind=kOutput, calls=%fused_computation | convolution fusion | flops 540016640 | bytes 7602176 | tf_op jit(solution)/shard_map/dot_general | solution.py:125
  121.8 0.0 copy-done.2
  (17 shorter events, 0.3 us)
Async XLA Ops:
  7.2 101.9 %all-gather.2.cloned.1.call-start = ((), (), s32[]{:S(2)}) async-start(), calls=%async_computation.6 | async-start | bytes 4259840 | tf_op jit(solution)/shard_map/all_gather | solution.py:87
  7.9 54.9 %copy-start.5 = (f32[32,256]{1,0:T(8,128)S(1)}, f32[32,256]{1,0:T(8,128)}, u32[]{:S(2)}) copy-start(f32[32,256]{1,0:T(8,128)} %param.12) | copy-start | bytes 98308
  7.9 54.9 %copy-start.4 = (f32[32,256]{1,0:T(8,128)S(1)}, f32[32,256]{1,0:T(8,128)}, u32[]{:S(2)}) copy-start(f32[32,256]{1,0:T(8,128)} %param.11) | copy-start | bytes 98308
  82.8 32.9 %copy-start = (bf16[512,256]{1,0:T(8,128)(2,1)S(1)}, bf16[512,256]{1,0:T(8,128)(2,1)}, u32[]{:S(2)}) copy-start(bf16[512,256]{1,0:T(8,128)(2,1)} %refs_2_.1) | copy-start | bytes 786436
  82.8 32.9 %copy-start.1 = (f32[32,512]{1,0:T(8,128)S(1)}, f32[32,512]{1,0:T(8,128)}, u32[]{:S(2)}) copy-start(f32[32,512]{1,0:T(8,128)} %param.9) | copy-start | bytes 196612
  115.6 6.2 %copy-start.2 = (f32[32,256]{1,0:T(8,128)}, f32[32,256]{1,0:T(8,128)S(1)}, u32[]{:S(2)}) copy-start(f32[32,256]{1,0:T(8,128)S(1)} %get-tuple-element.18) | copy-start | bytes 98308
  115.7 6.2 %copy-start.3 = (f32[32,256]{1,0:T(8,128)}, f32[32,256]{1,0:T(8,128)S(1)}, u32[]{:S(2)}) copy-start(f32[32,256]{1,0:T(8,128)S(1)} %get-tuple-element.17) | copy-start | bytes 98308
Sparse Core Ops, SparseCore 0:
  11.0 94.6 all-gather.1

commit v4 on v3

--- a/solution.py
+++ b/solution.py
@@ -62,7 +62,9 @@
     tokens, wide = saved_input.shape
     width = out_cotangent.shape[1]
     step, turned = 1024, 256
-    order = np.arange(turned).reshape(turned * fs // wide, tp, -1).transpose(1, 0, 2).reshape(-1)
+    lanes = lax.axis_size(TP[1])
+    order = np.arange(turned).reshape(turned * fs // wide, tp // lanes, lanes, -1)
+    order = order.transpose(2, 1, 0, 3).reshape(-1)
     turn = jnp.asarray(np.eye(turned, dtype=np.float32)[order], jnp.bfloat16)
     return pl.pallas_call(
         lambda *refs: projection_kernel(turned // tp, *refs),
@@ -88,8 +90,10 @@
     part = projected_part(saved_input, out_cotangent, factor, fs, tp)
     start = (lax.axis_index(TP) * mine).astype(jnp.uint32)
     part, start = lax.optimization_barrier((part, start))
-    tiles = exchanged(part, TP)
-    part = jnp.sum(tiles.astype(jnp.float32), axis=0).astype(jnp.bfloat16)
+    for axis in reversed(TP):
+        devices = lax.axis_size(axis)
+        tiles = exchanged(part.reshape(devices, -1, RANK), axis)
+        part = jnp.sum(tiles.astype(jnp.float32), axis=0).astype(jnp.bfloat16)
     tiles = exchanged(part.reshape(fs, mine, RANK), FS)
     own = jnp.sum(tiles.astype(jnp.float32), axis=0)
 

time: 129 us -> 129 us (level)
    all_to_all x6 -> x7, blocking collectives: 99.6 us -> 99 us  [exchanged(): return lax.all_to_all(blocks, axis, 0, 0, tiled=True)]
where the time goes in v4:
time: 129 us; the launch traced here: 128 us
  blocking collectives  99 us (77%)
  between operations  14.2 us (11%)
  Pallas kernels  6.17 us (5%)
  matrix products  5.41 us (4%)
  local copies, waits for them, and re-layouts  1.61 us (1%)
  other arithmetic  1.37 us (1%)
    all_to_all x7, blocking collectives, exchanged(): return lax.all_to_all(blocks, axis, 0, 0, tiled=True)  99 us
    pallas_call x1, Pallas kernels, projected_part(): pl.pallas_call(lambda *refs: projection_kernel(turned // tp, *refs), grid...  6.17 us
    dot_general x1, matrix products, on_device(): lax.dot_general(directions, factor, (((1,), (1,)), ((), ())), preferred_e...  4.25 us
  transfers between devices with their start and end apart: 1, of which 0 were waited for; matrix products, arithmetic and copies ran while one was open for 1% of the time, Pallas kernels for 5%

profile of v4, /device:TPU:1, one launch (start us, length us, event | category | flops | bytes accessed | tf_op | source)
XLA Modules:
  0.0 128.5 jit_solution(4516747429995958580)
XLA Ops:
  7.2 0.0 all-gather.2.cloned.1.call-start
  7.2 0.7 all-gather.2.cloned.1.call-update
  7.9 6.2 %projection.1 = bf16[8,256,256]{2,1,0:T(8,128)(2,1)} custom-call(bf16[1024,2048]{1,0:T(8,128)(2,1)} %refs_0_.1, bf16[1024,512]{1,0:T(8,128)(2,1)} %refs_1_.1, bf16[512,256]{1,0:T(8,128)(2,1)} %refs_2_.1, bf16[256,256]{1,0:T(8,128)(2,1)} %constant.13.clone.refs_3_), custom_call_target="tpu_custom_call" | custom-call | tf_op jit(solution)/shard_map/projection/pallas_call | solution.py:69
  14.1 12.3 %all_to_all.35 = bf16[2,1024,256]{2,1,0:T(8,128)(2,1)S(1)} all-to-all(bf16[2,1024,256]{2,1,0:T(8,128)(2,1)} %bitcast.11), channel_id=1, replica_groups=mesh['fs_0'=8,'fs_1'=8,'tp_0'=4,'tp_1'=2] {'tp_1'}, dimensions={0} | all-to-all | bytes 2097152 | tf_op jit(solution)/shard_map/all_to_all | solution.py:20
  26.4 0.5 reduce_sum.51
  26.9 11.6 %all_to_all.36 = bf16[4,256,256]{2,1,0:T(8,128)(2,1)S(1)} all-to-all(bf16[4,256,256]{2,1,0:T(8,128)(2,1)S(1)} %bitcast.13), channel_id=1, replica_groups=mesh['fs_0'=8,'fs_1'=8,'tp_0'=4,'tp_1'=2] {'tp_0'}, dimensions={0} | all-to-all | bytes 1048576 | tf_op jit(solution)/shard_map/all_to_all | solution.py:20
  38.5 0.1 reduce_sum.52
  38.6 23.3 %all_to_all.37 = bf16[64,4,256]{2,1,0:T(4,128)(2,1)S(1)} all-to-all(bf16[64,4,256]{2,1,0:T(4,128)(2,1)S(1)} %reshape.41), channel_id=1, replica_groups=mesh['fs_0'=8,'fs_1'=8,'tp_0'=4,'tp_1'=2] {'fs_0','fs_1'}, dimensions={0} | all-to-all | bytes 262144 | tf_op jit(solution)/shard_map/all_to_all | solution.py:20
  61.9 0.0 copy-done.5
  62.0 0.0 copy-done.4
  62.0 19.0 %all_to_all.38 = bf16[64,16,256]{2,1,0:T(8,128)(2,1)S(1)} all-to-all(bf16[64,16,256]{2,1,0:T(8,128)(2,1)S(1)} %broadcast_in_dim.12), channel_id=1, replica_groups=mesh['fs_0'=8,'fs_1'=8,'tp_0'=4,'tp_1'=2] {'fs_0','fs_1'}, dimensions={0} | all-to-all | bytes 1048576 | tf_op jit(solution)/shard_map/all_to_all | solution.py:20
  81.0 0.1 convert_element_type.38
  81.2 0.0 copy-start
  81.2 0.0 copy-start.1
  81.2 0.1 multiply_reduce_fusion
  81.3 15.8 %all_to_all.39 = f32[8,8,256]{2,1,0:T(8,128)S(1)} all-to-all(f32[8,8,256]{2,1,0:T(8,128)S(1)} %broadcast_in_dim.14), channel_id=1, replica_groups=mesh['fs_0'=8,'fs_1'=8,'tp_0'=4,'tp_1'=2] {'tp_0','tp_1'}, dimensions={0} | all-to-all | bytes 131072 | tf_op jit(solution)/shard_map/all_to_all | solution.py:20
  97.1 0.2 fusion.7
  97.3 0.4 fusion.6
  97.8 0.1 broadcast_in_dim.16
  97.9 11.0 %all_to_all.40 = bf16[4,64,4,256]{3,2,1,0:T(4,128)(2,1)S(1)} all-to-all(bf16[4,64,4,256]{3,2,1,0:T(4,128)(2,1)S(1)} %broadcast_in_dim.16), channel_id=1, replica_groups=mesh['fs_0'=8,'fs_1'=8,'tp_0'=4,'tp_1'=2] {'tp_0'}, dimensions={0} | all-to-all | bytes 1048576 | tf_op jit(solution)/shard_map/all_to_all | solution.py:20
  108.9 0.2 copy.21
  109.1 0.3 broadcast_in_dim.17
  109.3 6.1 %all_to_all.41 = bf16[2,4,64,4,256]{4,3,1,2,0:T(4,128)(2,1)S(1)} all-to-all(bf16[2,4,64,4,256]{4,3,1,2,0:T(4,128)(2,1)S(1)} %broadcast_in_dim.17), channel_id=1, replica_groups=mesh['fs_0'=8,'fs_1'=8,'tp_0'=4,'tp_1'=2] {'tp_1'}, dimensions={0} | all-to-all | bytes 2097152 | tf_op jit(solution)/shard_map/all_to_all | solution.py:20
  115.5 0.0 copy-start.2
  115.5 0.0 copy-start.3
  115.5 0.0 copy-done
  115.5 0.0 copy-done.1
  115.5 1.0 multiply_subtract_fusion
  116.5 0.6 copy.22
  117.1 0.3 reshape.43
  117.4 4.3 %subtract_convert_fusion = bf16[2048,512]{1,0:T(8,128)(2,1)} fusion(f32[2048,512]{1,0:T(8,128)} %all-gather.2.cloned.1.call-done, bf16[2048,256]{1,0:T(8,128)(2,1)S(1)} %reshape.43, bf16[512,256]{1,0:T(8,128)(2,1)S(1)} %copy-done), kind=kOutput, calls=%fused_computation | convolution fusion | flops 540016640 | bytes 7602176 | tf_op jit(solution)/shard_map/dot_general | solution.py:129
  121.6 0.0 copy-done.2
  (19 shorter events, 0.3 us)
Async XLA Ops:
  7.2 101.7 %all-gather.2.cloned.1.call-start = ((), (), s32[]{:S(2)}) async-start(), calls=%async_computation.7 | async-start | bytes 4259840 | tf_op jit(solution)/shard_map/all_gather | solution.py:89
  14.1 47.8 %copy-start.5 = (f32[32,256]{1,0:T(8,128)S(1)}, f32[32,256]{1,0:T(8,128)}, u32[]{:S(2)}) copy-start(f32[32,256]{1,0:T(8,128)} %param.12) | copy-start | bytes 98308
  14.1 47.9 %copy-start.4 = (f32[32,256]{1,0:T(8,128)S(1)}, f32[32,256]{1,0:T(8,128)}, u32[]{:S(2)}) copy-start(f32[32,256]{1,0:T(8,128)} %param.11) | copy-start | bytes 98308
  81.2 34.3 %copy-start = (bf16[512,256]{1,0:T(8,128)(2,1)S(1)}, bf16[512,256]{1,0:T(8,128)(2,1)}, u32[]{:S(2)}) copy-start(bf16[512,256]{1,0:T(8,128)(2,1)} %refs_2_.1) | copy-start | bytes 786436
  81.2 34.3 %copy-start.1 = (f32[32,512]{1,0:T(8,128)S(1)}, f32[32,512]{1,0:T(8,128)}, u32[]{:S(2)}) copy-start(f32[32,512]{1,0:T(8,128)} %param.9) | copy-start | bytes 196612
  115.5 6.2 %copy-start.2 = (f32[32,256]{1,0:T(8,128)}, f32[32,256]{1,0:T(8,128)S(1)}, u32[]{:S(2)}) copy-start(f32[32,256]{1,0:T(8,128)S(1)} %get-tuple-element.18) | copy-start | bytes 98308
  115.5 6.2 %copy-start.3 = (f32[32,256]{1,0:T(8,128)}, f32[32,256]{1,0:T(8,128)S(1)}, u32[]{:S(2)}) copy-start(f32[32,256]{1,0:T(8,128)S(1)} %get-tuple-element.17) | copy-start | bytes 98308
Sparse Core Ops, SparseCore 0:
  11.0 94.0 all-gather.1
